TPU v7x, 32 devices: a whole 2x2x4 slice. The times are simulated.
32 devices in a mesh: grp: 2 (over y), ra: 4 (over z), cb: 4 (over x, core).
Axes of the slice: x: 2, y: 2, z: 4, core: 2. Of those that a mesh axis runs over, the one named last changes fastest.
Arguments:
- tokens: bfloat16 [512, 4096], P('grp', 'cb'), parts along dimension 0, may hold values from -50 to 50
- norm_gains: float32 [3, 4096], P(None, 'cb'), may hold values from 0.1 to 1.9
- gate_weight: float32 [2, 4096, 11264], P(None, 'cb', 'ra'), may hold values from -0.09375 to 0.09375
- value_weight: float32 [2, 4096, 11264], P(None, 'cb', 'ra'), may hold values from -0.09375 to 0.09375
- gate_scale: float32 [2, 11264], P(None, 'ra'), may hold values from 0.3 to 3
- value_scale: float32 [2, 11264], P(None, 'ra'), may hold values from 0.3 to 3
- conv_gate: float32 [2, 3, 11264], P(None, None, 'ra'), may hold values from -3 to 3
- conv_value: float32 [2, 3, 11264], P(None, None, 'ra'), may hold values from -3 to 3
- down_weight: float32 [2, 11264, 4096], P(None, 'ra', 'cb'), may hold values from -0.07537784 to 0.07537784
- down_scale: float32 [2, 4096], P(None, 'cb'), may hold values from 0.3 to 3
Outputs:
- normed_out: bfloat16 [512, 4096], P('grp', 'cb'), parts along dimension 0
There are 2 independent parts, one for each index of `grp`. A program takes and returns all parts, laid end to end along the dimension named above; an argument that names none is the same for every part. Nothing has to cross between parts.
All inputs are finite; a program needn't handle non-finite values.
Results may differ from a plain program's by a relative error of at most 0.012.
The roundings to bfloat16 on the way count: a program that leaves them out, or rounds other values in their place, can miss the bound.
Values may be sent and summed in bfloat16 or wider, within the bound.
A program may use at most 192 MiB of HBM per device.

v0:
```python
import jax
import jax.numpy as jnp
from jax import lax
from jax.sharding import PartitionSpec as P

epsilon = 1e-06
residual_weight = 0.5


def causal_taps(projected, tap_weights):
    tap_count = tap_weights.shape[0]
    row_count = projected.shape[0]
    padded = jnp.pad(projected, ((tap_count - 1, 0), (0, 0)))
    result = jnp.zeros_like(projected)
    for tap_idx in range(tap_count):
        result = result + padded[tap_idx : tap_idx + row_count] * tap_weights[tap_idx]
    return result


def row_inverse(state_wide, model_width):
    squares = lax.psum(jnp.sum(state_wide * state_wide, axis=1, keepdims=True), "cb")
    return lax.rsqrt(squares / model_width + epsilon)


def on_device(
    tokens,
    norm_gains,
    gate_weight,
    value_weight,
    gate_scale,
    value_scale,
    conv_gate,
    conv_value,
    down_weight,
    down_scale,
):
    model_width = lax.axis_size("cb") * tokens.shape[1]
    layer_count = gate_weight.shape[0]
    current = tokens
    for layer_idx in range(layer_count):
        state_wide = current.astype(jnp.float32)
        inverse = row_inverse(state_wide, model_width)
        scaled = (state_wide * norm_gains[layer_idx]).astype(jnp.bfloat16)
        gate_part = jnp.dot(
            scaled, gate_weight[layer_idx].astype(jnp.bfloat16), preferred_element_type=jnp.float32
        )
        value_part = jnp.dot(
            scaled, value_weight[layer_idx].astype(jnp.bfloat16), preferred_element_type=jnp.float32
        )
        gate_sum, value_sum = (
            lax.psum_scatter(gate_part, "cb", scatter_dimension=1, tiled=True),
            lax.psum_scatter(value_part, "cb", scatter_dimension=1, tiled=True),
        )
        share_cols = gate_sum.shape[1]
        first_col = lax.axis_index("cb") * share_cols
        gate_cols = lax.dynamic_slice_in_dim(gate_scale[layer_idx], first_col, share_cols, 0)
        value_cols = lax.dynamic_slice_in_dim(value_scale[layer_idx], first_col, share_cols, 0)
        gate_taps = lax.dynamic_slice_in_dim(conv_gate[layer_idx], first_col, share_cols, 1)
        value_taps = lax.dynamic_slice_in_dim(conv_value[layer_idx], first_col, share_cols, 1)
        gate_pre = inverse * gate_cols * gate_sum
        value_pre = inverse * value_cols * value_sum
        hidden = (
            jax.nn.gelu(causal_taps(gate_pre, gate_taps), approximate=True)
            * causal_taps(value_pre, value_taps)
        ).astype(jnp.bfloat16)
        hidden = lax.all_gather(hidden, "cb", axis=1, tiled=True)
        partial_value = jnp.dot(
            hidden, down_weight[layer_idx].astype(jnp.bfloat16), preferred_element_type=jnp.float32
        )
        down_total = lax.psum(partial_value, "ra")
        current = (residual_weight * state_wide + down_scale[layer_idx] * down_total).astype(
            jnp.bfloat16
        )
    state_wide = current.astype(jnp.float32)
    inverse = row_inverse(state_wide, model_width)
    return (state_wide * inverse * norm_gains[layer_count]).astype(jnp.bfloat16)


def solution(mesh):
    in_specs = (
        P("grp", "cb"),
        P(None, "cb"),
        P(None, "cb", "ra"),
        P(None, "cb", "ra"),
        P(None, "ra"),
        P(None, "ra"),
        P(None, None, "ra"),
        P(None, None, "ra"),
        P(None, "ra", "cb"),
        P(None, "cb"),
    )
    out_specs = P("grp", "cb")
    return jax.shard_map(
        on_device, mesh=mesh, in_specs=in_specs, out_specs=out_specs, check_vma=False
    )
```

profile of v0, /device:TPU:0, one launch (start us, length us, event | category | flops | bytes accessed | tf_op | source)
XLA Modules:
  0.0 362.3 jit_solution(13226815253919093914)
XLA Ops:
  6.5 0.8 fusion.77
  7.4 8.6 %convert.12 = bf16[2,1024,2816]{2,1,0:T(8,128)(2,1)S(1)} convert(f32[2,1024,2816]{2,1,0:T(8,128)} %param.12) | non-fusion elementwise | flops 5767168 | bytes 34603008 | tf_op jit(solution)/shard_map/convert.5
  16.0 4.2 %copy-done.1 = bf16[2,1024,2816]{2,1,0:T(8,128)(2,1)} copy-done((bf16[2,1024,2816]{2,1,0:T(8,128)(2,1)}, bf16[2,1024,2816]{2,1,0:T(8,128)(2,1)S(1)}, u32[]{:S(2)}) %copy-start.1) | copy-done | bytes 11534360
  20.2 4.1 %fusion.5 = f32[256,2816]{0,1:T(8,128)} fusion(bf16[2,1024,2816]{2,1,0:T(8,128)(2,1)S(1)} %convert.12, bf16[256,1024]{1,0:T(8,128)(2,1)S(1)} %copy-done.2, f32[1024]{0:T(1024)S(1)} %bitcast.42), kind=kOutput, calls=%fused_computation.11 | convolution fusion | flops 1477181440 | bytes 9179136 | tf_op jit(solution)/shard_map/dot_general | solution.py:44
  24.4 8.6 %convert.13 = bf16[2,1024,2816]{2,1,0:T(8,128)(2,1)S(1)} convert(f32[2,1024,2816]{2,1,0:T(8,128)} %param.13) | non-fusion elementwise | flops 5767168 | bytes 34603008 | tf_op jit(solution)/shard_map/convert.4
  32.9 4.8 %copy-done = bf16[2,1024,2816]{2,1,0:T(8,128)(2,1)} copy-done((bf16[2,1024,2816]{2,1,0:T(8,128)(2,1)}, bf16[2,1024,2816]{2,1,0:T(8,128)(2,1)S(1)}, u32[]{:S(2)}) %copy-start) | copy-done | bytes 11534360
  37.8 4.0 %fusion.4 = f32[256,2816]{0,1:T(8,128)} fusion(bf16[2,1024,2816]{2,1,0:T(8,128)(2,1)S(1)} %convert.13, bf16[256,1024]{1,0:T(8,128)(2,1)S(1)} %copy-done.2, f32[1024]{0:T(1024)S(1)} %bitcast.43), kind=kOutput, calls=%fused_computation.9 | convolution fusion | flops 1477181440 | bytes 9179136 | tf_op jit(solution)/shard_map/dot_general | solution.py:47
  42.0 0.2 fusion.11
  42.2 9.0 %psum.35 = f32[256,1]{0,1:T(1,128)S(1)} all-reduce(f32[256,1]{0,1:T(1,128)S(1)} %bitcast.39), channel_id=1, replica_groups=mesh['grp'=2,'ra'=4,'cb'=4] {'cb'}, use_global_device_ids=true, to_apply=%region_1.0 | all-reduce | flops 256 | bytes 2048 | tf_op jit(solution)/shard_map/psum | solution.py:21
  51.5 12.1 %reduce-scatter.5.cloned.1.call-done = f32[256,704]{0,1:T(8,128)} async-done(((f32[256,2816]{0,1:T(8,128)}), f32[256,704]{0,1:T(8,128)}) %reduce-scatter.5.cloned.1.call-update) | async-done | bytes 720912 | tf_op jit(solution)/shard_map/reduce_scatter | solution.py:51
  63.5 38.8 %reduce-scatter.7.cloned.1.call-done = f32[256,704]{0,1:T(8,128)} async-done(((f32[256,2816]{0,1:T(8,128)}), f32[256,704]{0,1:T(8,128)}) %reduce-scatter.7.cloned.1.call-update) | async-done | bytes 720912 | tf_op jit(solution)/shard_map/reduce_scatter | solution.py:52
  102.3 1.6 multiply_multiply_fusion.4
  103.9 2.2 fusion.25
  106.2 12.6 %convert.14 = bf16[2,2816,1024]{2,1,0:T(8,128)(2,1)} convert(f32[2,2816,1024]{2,1,0:T(8,128)} %param.18) | non-fusion elementwise | flops 5767168 | bytes 34603008 | tf_op jit(solution)/shard_map/convert.3
  118.8 6.4 %all-gather.3.cloned.1.call-done = bf16[256,2816]{0,1:T(8,128)(2,1)} async-done(((bf16[256,704]{0,1:T(8,128)(2,1)}), bf16[256,2816]{0,1:T(8,128)(2,1)}) %all-gather.3.cloned.1.call-update) | async-done | bytes 1441808 | tf_op jit(solution)/shard_map/all_gather | solution.py:66
  125.2 5.8 %fusion.3 = f32[256,1024]{1,0:T(8,128)} fusion(bf16[256,2816]{0,1:T(8,128)(2,1)} %all-gather.3.cloned.1.call-done, bf16[2,2816,1024]{2,1,0:T(8,128)(2,1)} %convert.14), kind=kOutput, calls=%fused_computation.7 | convolution fusion | flops 1476395008 | bytes 8257536 | tf_op jit(solution)/shard_map/dot_general | solution.py:67
  131.0 52.0 %all-reduce.7.cloned.1.call-done = f32[256,1024]{1,0:T(8,128)} async-done(((f32[256,1024]{1,0:T(8,128)}), f32[256,1024]{1,0:T(8,128)}) %all-reduce.7.cloned.1.call-update) | async-done | bytes 1048592 | tf_op jit(solution)/shard_map/psum | solution.py:70
  183.0 1.5 fusion.15
  184.5 6.6 %fusion.2 = f32[256,2816]{0,1:T(8,128)} fusion(bf16[2,1024,2816]{2,1,0:T(8,128)(2,1)} %copy-done.1, bf16[256,1024]{1,0:T(8,128)(2,1)S(1)} %get-tuple-element.20, f32[1024]{0:T(1024)S(1)} %bitcast.40), kind=kOutput, calls=%fused_computation.5 | convolution fusion | flops 1477181440 | bytes 9179136 | tf_op jit(solution)/shard_map/dot_general | solution.py:44
  191.2 0.2 reduce-scatter.11.cloned.1.call-start
  191.4 6.6 %fusion.1 = f32[256,2816]{0,1:T(8,128)} fusion(bf16[2,1024,2816]{2,1,0:T(8,128)(2,1)} %copy-done, bf16[256,1024]{1,0:T(8,128)(2,1)S(1)} %get-tuple-element.20, f32[1024]{0:T(1024)S(1)} %bitcast.41), kind=kOutput, calls=%fused_computation.3 | convolution fusion | flops 1477181440 | bytes 9179136 | tf_op jit(solution)/shard_map/dot_general | solution.py:47
  198.3 6.8 %psum.37 = f32[256,1]{0,1:T(1,128)S(1)} all-reduce(f32[256,1]{0,1:T(1,128)S(1)} %bitcast.34), channel_id=1, replica_groups=mesh['grp'=2,'ra'=4,'cb'=4] {'cb'}, use_global_device_ids=true, to_apply=%region_6.7 | all-reduce | flops 256 | bytes 2048 | tf_op jit(solution)/shard_map/psum | solution.py:21
  205.2 21.6 %reduce-scatter.9.cloned.1.call-done = f32[256,704]{0,1:T(8,128)} async-done(((f32[256,2816]{0,1:T(8,128)}), f32[256,704]{0,1:T(8,128)}) %reduce-scatter.9.cloned.1.call-update) | async-done | bytes 720912 | tf_op jit(solution)/shard_map/reduce_scatter | solution.py:51
  226.8 38.6 %reduce-scatter.11.cloned.1.call-done = f32[256,704]{0,1:T(8,128)} async-done(((f32[256,2816]{0,1:T(8,128)}), f32[256,704]{0,1:T(8,128)}) %reduce-scatter.11.cloned.1.call-update) | async-done | bytes 720912 | tf_op jit(solution)/shard_map/reduce_scatter | solution.py:52
  265.4 1.6 multiply_multiply_fusion.2
  267.0 2.2 fusion.34
  269.3 19.0 %all-gather.5.cloned.1.call-done = bf16[256,2816]{0,1:T(8,128)(2,1)} async-done(((bf16[256,704]{0,1:T(8,128)(2,1)}), bf16[256,2816]{0,1:T(8,128)(2,1)}) %all-gather.5.cloned.1.call-update) | async-done | bytes 1441808 | tf_op jit(solution)/shard_map/all_gather | solution.py:66
  288.3 5.7 %fusion = f32[256,1024]{1,0:T(8,128)} fusion(bf16[256,2816]{0,1:T(8,128)(2,1)} %all-gather.5.cloned.1.call-done, bf16[2,2816,1024]{2,1,0:T(8,128)(2,1)} %convert.14), kind=kOutput, calls=%fused_computation.1 | convolution fusion | flops 1476395008 | bytes 8257536 | tf_op jit(solution)/shard_map/dot_general | solution.py:67
  294.0 52.1 %all-reduce.9.cloned.1.call-done = f32[256,1024]{1,0:T(8,128)} async-done(((f32[256,1024]{1,0:T(8,128)}), f32[256,1024]{1,0:T(8,128)}) %all-reduce.9.cloned.1.call-update) | async-done | bytes 1048592 | tf_op jit(solution)/shard_map/psum | solution.py:70
  346.1 1.5 fusion.6
  347.6 6.8 %psum.39 = f32[256,1]{0,1:T(1,128)S(1)} all-reduce(f32[256,1]{0,1:T(1,128)S(1)} %bitcast.37), channel_id=1, replica_groups=mesh['grp'=2,'ra'=4,'cb'=4] {'cb'}, use_global_device_ids=true, to_apply=%region_11.12 | all-reduce | flops 256 | bytes 2048 | tf_op jit(solution)/shard_map/psum | solution.py:21
  354.5 1.0 fusion.8
  (41 shorter events, 1.0 us)
Async XLA Ops:
  6.5 57.0 %reduce-scatter.5.cloned.1.call-start = ((), (), s32[]{:S(2)}) async-start(), calls=%async_computation.4 | async-start | bytes 3604480 | tf_op jit(solution)/shard_map/reduce_scatter | solution.py:51
  7.4 12.8 %copy-start.2 = (bf16[256,1024]{1,0:T(8,128)(2,1)S(1)}, bf16[256,1024]{1,0:T(8,128)(2,1)}, u32[]{:S(2)}) copy-start(bf16[256,1024]{1,0:T(8,128)(2,1)} %param.10) | copy-start | bytes 1572868
  16.0 4.2 %copy-start.1 = (bf16[2,1024,2816]{2,1,0:T(8,128)(2,1)}, bf16[2,1024,2816]{2,1,0:T(8,128)(2,1)S(1)}, u32[]{:S(2)}) copy-start(bf16[2,1024,2816]{2,1,0:T(8,128)(2,1)S(1)} %convert.12) | copy-start | bytes 34603012
  24.3 78.0 %reduce-scatter.7.cloned.1.call-start = ((), (), s32[]{:S(2)}) async-start(), calls=%async_computation.5 | async-start | bytes 3604480 | tf_op jit(solution)/shard_map/reduce_scatter | solution.py:52
  32.9 4.8 %copy-start = (bf16[2,1024,2816]{2,1,0:T(8,128)(2,1)}, bf16[2,1024,2816]{2,1,0:T(8,128)(2,1)S(1)}, u32[]{:S(2)}) copy-start(bf16[2,1024,2816]{2,1,0:T(8,128)(2,1)S(1)} %convert.13) | copy-start | bytes 34603012
  37.7 4.1 %copy-start.5 = (f32[2,2816]{1,0:T(2,128)S(1)}, f32[2,2816]{1,0:T(2,128)}, u32[]{:S(2)}) copy-start(f32[2,2816]{1,0:T(2,128)} %param.14) | copy-start | bytes 67588
  37.7 4.1 %copy-start.6 = (f32[2,2816]{1,0:T(2,128)S(1)}, f32[2,2816]{1,0:T(2,128)}, u32[]{:S(2)}) copy-start(f32[2,2816]{1,0:T(2,128)} %param.15) | copy-start | bytes 67588
  37.8 13.5 %copy-start.3 = (f32[2,3,2816]{2,0,1:T(2,128)S(1)}, f32[2,3,2816]{2,0,1:T(2,128)}, u32[]{:S(2)}) copy-start(f32[2,3,2816]{2,0,1:T(2,128)} %param.16) | copy-start | bytes 202756
  37.8 13.5 %copy-start.4 = (f32[2,3,2816]{2,0,1:T(2,128)S(1)}, f32[2,3,2816]{2,0,1:T(2,128)}, u32[]{:S(2)}) copy-start(f32[2,3,2816]{2,0,1:T(2,128)} %param.17) | copy-start | bytes 202756
  41.8 83.4 %all-gather.3.cloned.1.call-start = ((), (), s32[]{:S(2)}) async-start(), calls=%async_computation.6 | async-start | bytes 1802240 | tf_op jit(solution)/shard_map/all_gather | solution.py:66
  106.1 76.9 %all-reduce.7.cloned.1.call-start = ((), (), s32[]{:S(2)}) async-start(), calls=%async_computation.7 | async-start | bytes 2097152 | tf_op jit(solution)/shard_map/psum | solution.py:70
  118.8 12.2 %copy-start.7 = (f32[2,1024]{1,0:T(2,128)S(1)}, f32[2,1024]{1,0:T(2,128)}, u32[]{:S(2)}) copy-start(f32[2,1024]{1,0:T(2,128)} %param.19) | copy-start | bytes 24580
  130.9 95.8 %reduce-scatter.9.cloned.1.call-start = ((), (), s32[]{:S(2)}) async-start(), calls=%async_computation.8 | async-start | bytes 3604480 | tf_op jit(solution)/shard_map/reduce_scatter | solution.py:51
  191.2 74.2 %reduce-scatter.11.cloned.1.call-start = ((), (), s32[]{:S(2)}) async-start(), calls=%async_computation.9 | async-start | bytes 3604480 | tf_op jit(solution)/shard_map/reduce_scatter | solution.py:52
  198.1 90.2 %all-gather.5.cloned.1.call-start = ((), (), s32[]{:S(2)}) async-start(), calls=%async_computation.10 | async-start | bytes 1802240 | tf_op jit(solution)/shard_map/all_gather | solution.py:66
  269.2 76.9 %all-reduce.9.cloned.1.call-start = ((), (), s32[]{:S(2)}) async-start(), calls=%async_computation.11 | async-start | bytes 2097152 | tf_op jit(solution)/shard_map/psum | solution.py:70
Sparse Core Ops, SparseCore 0:
  24.4 39.0 reduce-scatter.4
  66.1 36.1 reduce-scatter.6
  106.2 18.8 all-gather.2
  131.1 51.8 all-reduce.6
  191.3 35.4 reduce-scatter.8
  229.2 36.1 reduce-scatter.10
  269.3 18.8 all-gather.4
  294.1 51.8 all-reduce.8
where the time goes:
time: 363 us; the launch traced here: 362 us
  waiting for transfers between devices  241 us (66%)
  other arithmetic  41.6 us (11%)
  matrix products  32.8 us (9%)
  blocking collectives  22.7 us (6%)
  between operations  13.7 us (4%)
  local copies, waits for them, and re-layouts  10.5 us (3%)
    psum x2, waiting for transfers between devices, on_device(): down_total = lax.psum(partial_value, 'ra')  104 us
    reduce_scatter x2, waiting for transfers between devices, on_device(): lax.psum_scatter(value_part, 'cb', scatter_dimension=1, tiled=True)  77.4 us
    reduce_scatter x2, waiting for transfers between devices, on_device(): lax.psum_scatter(gate_part, 'cb', scatter_dimension=1, tiled=True)  33.6 us
    another operation x3, other arithmetic  29.8 us
    all_gather x2, waiting for transfers between devices, on_device(): hidden = lax.all_gather(hidden, 'cb', axis=1, tiled=True)  25.4 us
    psum x3, blocking collectives, row_inverse(): lax.psum(jnp.sum(state_wide * state_wide, axis=1, keepdims=True), 'cb')  22.7 us
    dot_general x2, matrix products, on_device(): jnp.dot(hidden, down_weight[layer_idx].astype(jnp.bfloat16), preferred_el...  11.5 us
    dot_general x2, matrix products, on_device(): jnp.dot(scaled, gate_weight[layer_idx].astype(jnp.bfloat16), preferred_el...  10.7 us
  transfers between devices with their start and end apart: 8, of which 8 were waited for; matrix products, arithmetic and copies ran while one was open for 9% of the time, Pallas kernels for 0%

commit v1 on v0

--- a/solution.py
+++ b/solution.py
@@ -1,6 +1,10 @@
+import functools
+
 import jax
 import jax.numpy as jnp
 from jax import lax
+from jax.experimental import pallas as pl
+from jax.experimental.pallas import tpu as pltpu
 from jax.sharding import PartitionSpec as P
 
 epsilon = 1e-06
@@ -76,6 +80,477 @@
     return (state_wide * inverse * norm_gains[layer_count]).astype(jnp.bfloat16)
 
 
+HALVES = 2
+CORES = 2
+LANES = 128
+CHUNK = 256
+RING = 12
+STAGED = 5
+BUBBLES = 4
+PAIR_SUM, GATED, PAIR_GATHER, DOWN = 1, 4, 7, 8
+Z_SUM, Z_GATHER, Z_SCALE = 4, 7, 8
+
+
+def fused_kernel(
+    ra_count,
+    cb_count,
+    tokens,
+    gains,
+    gate_hbm,
+    value_hbm,
+    gate_scale,
+    value_scale,
+    conv_gate,
+    conv_value,
+    down_hbm,
+    down_scale,
+    out,
+    gate_stage,
+    value_stage,
+    down_stage,
+    wide_weight,
+    down_weight,
+    current,
+    scaled,
+    inverse,
+    padded,
+    carry,
+    pair_send,
+    pair_recv,
+    pair_own,
+    x_send,
+    x_recv,
+    hidden,
+    acc,
+    z_send,
+    z_recv,
+    z_own,
+    sq_send,
+    sq_recv,
+    gate_sem,
+    value_sem,
+    down_sem,
+    pair_ss,
+    pair_rs,
+    x_ss,
+    x_rs,
+    hx_ss,
+    hx_rs,
+    hp_ss,
+    hp_rs,
+    z_ss,
+    z_rs,
+    c_ss,
+    c_rs,
+    sq_ss,
+    sq_rs,
+):
+    f32, bf16 = jnp.float32, jnp.bfloat16
+    layers = gate_hbm.shape[0]
+    chunks = gate_hbm.shape[2] // CHUNK
+    taps = conv_gate.shape[1]
+    rows = tokens.shape[1]
+    width = tokens.shape[2]
+    model_width = width * cb_count
+    x_count = cb_count // CORES
+    block = rows // cb_count
+    z_block = rows // ra_count
+    period = HALVES * chunks + BUBBLES
+    last_item = layers * period - BUBBLES
+    streamed = layers * chunks
+
+    me_cb = lax.axis_index("cb")
+    me_ra = lax.axis_index("ra")
+    me_x, me_core = lax.div(me_cb, CORES), lax.rem(me_cb, CORES)
+    partner = me_x * CORES + (1 - me_core)
+
+    def others(count, me):
+        return [lax.rem(me + step, count) for step in range(1, count)]
+
+    def remote(src, dst, send, recv, axis, index):
+        return pltpu.make_async_remote_copy(
+            src_ref=src,
+            dst_ref=dst,
+            send_sem=send,
+            recv_sem=recv,
+            device_id={axis: index},
+            device_id_type=pl.DeviceIdType.MESH,
+        )
+
+    def cb_of(x_index):
+        return x_index * CORES + me_core
+
+    def wide_copies(n):
+        layer, chunk, slot = lax.div(n, chunks), lax.rem(n, chunks), lax.rem(n, STAGED)
+        cols = pl.ds(pl.multiple_of(chunk * CHUNK, CHUNK), CHUNK)
+        return (
+            pltpu.make_async_copy(gate_hbm.at[layer, :, cols], gate_stage.at[slot], gate_sem.at[slot]),
+            pltpu.make_async_copy(value_hbm.at[layer, :, cols], value_stage.at[slot], value_sem.at[slot]),
+        )
+
+    def down_copy(n):
+        layer, chunk, slot = lax.div(n, chunks), lax.rem(n, chunks), lax.rem(n, STAGED)
+        cols = pl.ds(pl.multiple_of(chunk * CHUNK, CHUNK), CHUNK)
+        return pltpu.make_async_copy(down_hbm.at[layer, cols, :], down_stage.at[slot], down_sem.at[slot])
+
+    for n in range(min(STAGED, streamed)):
+        for copy in wide_copies(n):
+            copy.start()
+        down_copy(n).start()
+
+    barrier = pltpu.get_barrier_semaphore()
+    for axis, count, me in (("cb", cb_count, me_cb), ("ra", ra_count, me_ra)):
+        for peer in others(count, me):
+            pl.semaphore_signal(
+                barrier, inc=1, device_id={axis: peer}, device_id_type=pl.DeviceIdType.MESH
+            )
+    pl.semaphore_wait(barrier, cb_count + ra_count - 2)
+
+    def pair_copy(slot):
+        return remote(
+            pair_send.at[slot], pair_recv.at[slot], pair_ss.at[slot], pair_rs.at[slot], "cb", partner
+        )
+
+    def x_copy(slot, peer, source):
+        return remote(
+            x_send.at[slot, peer],
+            x_recv.at[slot, source],
+            x_ss.at[slot, peer],
+            x_rs.at[slot, source],
+            "cb",
+            cb_of(peer),
+        )
+
+    def hx_copy(slot, peer, source):
+        place = hidden.at[slot, me_core * x_count + source]
+        return remote(place, place, hx_ss.at[slot, peer], hx_rs.at[slot, source], "cb", cb_of(peer))
+
+    def hp_copy(slot, core):
+        place = hidden.at[slot, pl.ds(core * x_count, x_count)]
+        return remote(place, place, hp_ss.at[slot], hp_rs.at[slot], "cb", partner)
+
+    def z_copy(part, peer, source):
+        return remote(
+            z_send.at[part, peer],
+            z_recv.at[part, source],
+            z_ss.at[part, peer],
+            z_rs.at[part, source],
+            "ra",
+            peer,
+        )
+
+    def c_copy(part, layer, half, peer, source):
+        place = current.at[layer, half, source]
+        return remote(place, place, c_ss.at[part, peer], c_rs.at[part, source], "ra", peer)
+
+    def sq_copy(event, peer, source):
+        return remote(
+            sq_send.at[event], sq_recv.at[event, source], sq_ss.at[event, peer], sq_rs.at[event, source], "cb", peer
+        )
+
+    def scale_rows(layer, half):
+        event = layer * HALVES + half
+        wide = current[layer, half].reshape(rows, width).astype(f32)
+        scaled[half] = (wide * gains[pl.ds(layer, 1), :]).astype(bf16)
+        squares = jnp.sum(wide * wide, axis=1, keepdims=True)
+        sq_send[event] = jnp.broadcast_to(squares, (rows, LANES)).T[:8]
+        for peer in others(cb_count, me_cb):
+            sq_copy(event, peer, me_cb).start()
+
+    def finish_squares(layer, half):
+        event = layer * HALVES + half
+        total = sq_send[event]
+        for peer in others(cb_count, me_cb):
+            copy = sq_copy(event, peer, peer)
+            copy.wait_send()
+            copy.wait_recv()
+            total = total + sq_recv[event, peer]
+        row = lax.rsqrt(total / model_width + epsilon)
+        inverse[half] = jnp.broadcast_to(row[:1], (LANES, rows)).T
+
+    for half in range(HALVES):
+        current[0, half] = tokens[half].reshape(ra_count, z_block, width)
+        scale_rows(0, half)
+    for half in range(HALVES):
+        finish_squares(0, half)
+
+    def place_of(item):
+        layer, rest = lax.div(item, period), lax.rem(item, period)
+        half, chunk = lax.div(rest, chunks), lax.rem(rest, chunks)
+        ordinal = layer * (HALVES * chunks) + rest
+        return layer, half, chunk, lax.rem(ordinal, RING)
+
+    def project(layer, half, chunk, slot):
+        n = layer * chunks + chunk
+
+        @pl.when(half == 0)
+        def _():
+            stage = lax.rem(n, STAGED)
+            for copy in wide_copies(n):
+                copy.wait()
+            wide_weight[chunk, :, :CHUNK] = gate_stage[stage].astype(bf16)
+            wide_weight[chunk, :, CHUNK:] = value_stage[stage].astype(bf16)
+
+            @pl.when(n + STAGED < streamed)
+            def _():
+                for copy in wide_copies(n + STAGED):
+                    copy.start()
+
+        product = jnp.dot(scaled[half], wide_weight[chunk], preferred_element_type=f32)
+        inv = inverse[half]
+        cols = pl.ds(pl.multiple_of(chunk * CHUNK, CHUNK), CHUNK)
+        one = pl.ds(layer, 1)
+        scales = jnp.concatenate([gate_scale[one, cols], value_scale[one, cols]], axis=1)
+        weights = jnp.concatenate([conv_gate[layer, :, cols], conv_value[layer, :, cols]], axis=1)
+        wide_inv = jnp.concatenate([inv] * (2 * CHUNK // LANES), axis=1)
+        pre = product * wide_inv * scales
+        before = carry[chunk]
+        padded[:8] = jnp.where(half == 0, jnp.zeros_like(before), before)
+        padded[8:] = pre
+        carry[chunk] = pre[rows - 8 :]
+        total = jnp.zeros_like(pre)
+        for tap in range(taps):
+            total = total + padded[pl.ds(8 - (taps - 1) + tap, rows), :] * weights[tap : tap + 1]
+        part = rows // CORES
+        for core in range(CORES):
+            piece = total[core * part : (core + 1) * part]
+
+            @pl.when(me_core == core)
+            def _():
+                pair_own[slot] = piece.reshape(x_count, block, 2 * CHUNK)
+
+            @pl.when(me_core != core)
+            def _():
+                pair_send[slot] = piece.astype(bf16).reshape(x_count, block, 2 * CHUNK)
+
+        pair_copy(slot).start()
+
+    def pair_sum(layer, half, chunk, slot):
+        pair_copy(slot).wait()
+        both = pair_own[slot] + pair_recv[slot].astype(f32)
+        pair_own[slot] = both
+        x_send[slot] = both.astype(bf16)
+        for peer in others(x_count, me_x):
+            x_copy(slot, peer, me_x).start()
+
+    def gated(layer, half, chunk, slot):
+        total = pair_own[slot, me_x]
+        for peer in others(x_count, me_x):
+            copy = x_copy(slot, peer, peer)
+            copy.wait_send()
+            copy.wait_recv()
+            total = total + x_recv[slot, peer].astype(f32)
+        unit = jax.nn.gelu(total[:, :CHUNK], approximate=True) * total[:, CHUNK:]
+        hidden[slot, me_core * x_count + me_x] = unit.astype(bf16)
+        for peer in others(x_count, me_x):
+            hx_copy(slot, peer, me_x).start()
+
+    def pair_gather(layer, half, chunk, slot):
+        for peer in others(x_count, me_x):
+            hx_copy(slot, peer, me_x).wait_send()
+            hx_copy(slot, peer, peer).wait_recv()
+        hp_copy(slot, me_core).start()
+
+    def project_down(layer, half, chunk, slot):
+        n = layer * chunks + chunk
+
+        @pl.when(half == 0)
+        def _():
+            stage = lax.rem(n, STAGED)
+            down_copy(n).wait()
+            down_weight[chunk] = down_stage[stage].astype(bf16)
+
+            @pl.when(n + STAGED < streamed)
+            def _():
+                down_copy(n + STAGED).start()
+
+        hp_copy(slot, me_core).wait_send()
+        hp_copy(slot, 1 - me_core).wait_recv()
+        product = jnp.dot(
+            hidden[slot].reshape(rows, CHUNK), down_weight[chunk], preferred_element_type=f32
+        ).reshape(ra_count, z_block, width)
+
+        @pl.when(chunk == 0)
+        def _():
+            acc[...] = product
+
+        @pl.when(chunk > 0)
+        def _():
+            acc[...] += product
+
+        @pl.when(chunk == chunks - 1)
+        def _():
+            part = layer * HALVES + half
+            z_send[part] = acc[...].astype(bf16)
+            z_own[part] = acc[me_ra]
+            for peer in others(ra_count, me_ra):
+                z_copy(part, peer, me_ra).start()
+
+    def z_sum(layer, half, chunk, slot):
+        part = layer * HALVES + half
+        total = z_own[part]
+        for peer in others(ra_count, me_ra):
+            copy = z_copy(part, peer, peer)
+            copy.wait_send()
+            copy.wait_recv()
+            total = total + z_recv[part, peer].astype(f32)
+        kept = residual_weight * current[layer, half, me_ra].astype(f32)
+        current[layer + 1, half, me_ra] = (kept + down_scale[pl.ds(layer, 1), :] * total).astype(bf16)
+        for peer in others(ra_count, me_ra):
+            c_copy(part, layer + 1, half, peer, me_ra).start()
+
+    def z_gather(layer, half, chunk, slot):
+        part = layer * HALVES + half
+        for peer in others(ra_count, me_ra):
+            c_copy(part, layer + 1, half, peer, me_ra).wait_send()
+            c_copy(part, layer + 1, half, peer, peer).wait_recv()
+        scale_rows(layer + 1, half)
+
+    def z_scale(layer, half, chunk, slot):
+        finish_squares(layer + 1, half)
+
+        @pl.when(layer == layers - 1)
+        def _():
+            wide = current[layers, half].reshape(rows, width).astype(f32)
+            inv = jnp.concatenate([inverse[half]] * (width // LANES), axis=1)
+            out[half] = (wide * inv * gains[pl.ds(layers, 1), :]).astype(bf16)
+
+    stages = (
+        (DOWN + Z_SCALE, True, z_scale),
+        (DOWN + Z_GATHER, True, z_gather),
+        (DOWN + Z_SUM, True, z_sum),
+        (PAIR_GATHER, False, pair_gather),
+        (GATED, False, gated),
+        (PAIR_SUM, False, pair_sum),
+        (0, False, project),
+        (DOWN, False, project_down),
+    )
+    assert DOWN + Z_SCALE <= chunks + BUBBLES + 1
+
+    def step(index, _):
+        for delay, at_end, stage in stages:
+            item = index - delay
+            rest = lax.rem(item + period, period)
+            valid = (item >= 0) & (item < last_item) & (rest < HALVES * chunks)
+            if at_end:
+                valid = valid & (lax.rem(rest, chunks) == chunks - 1)
+
+            @pl.when(valid)
+            def _(stage=stage, item=item):
+                stage(*place_of(item))
+
+        return 0
+
+    lax.fori_loop(0, last_item + DOWN + Z_SCALE, step, 0)
+
+
+def fits(ra_count, cb_count, tokens, gate_weight, conv_gate):
+    rows = tokens.shape[0] // HALVES
+    return (
+        cb_count % CORES == 0
+        and cb_count > CORES
+        and ra_count > 1
+        and tokens.shape[0] % HALVES == 0
+        and rows % LANES == 0
+        and (rows // LANES) == 1
+        and rows % (16 * cb_count) == 0
+        and rows % (16 * ra_count) == 0
+        and tokens.shape[1] % LANES == 0
+        and gate_weight.shape[2] % CHUNK == 0
+        and gate_weight.shape[2] // CHUNK + BUBBLES + 1 >= DOWN + Z_SCALE
+        and conv_gate.shape[1] <= 9
+    )
+
+
+def on_device_any(ra_count, cb_count, *args):
+    (
+        tokens,
+        norm_gains,
+        gate_weight,
+        value_weight,
+        gate_scale,
+        value_scale,
+        conv_gate,
+        conv_value,
+        down_weight,
+        down_scale,
+    ) = args
+    if not fits(ra_count, cb_count, tokens, gate_weight, conv_gate):
+        return on_device(*args)
+    f32, bf16 = jnp.float32, jnp.bfloat16
+    layers, width, units = gate_weight.shape
+    rows = tokens.shape[0] // HALVES
+    chunks = units // CHUNK
+    x_count = cb_count // CORES
+    block, z_block = rows // cb_count, rows // ra_count
+    parts, events = layers * HALVES, (layers + 1) * HALVES
+    vmem, dma = pltpu.VMEM, pltpu.SemaphoreType.DMA
+    in_vmem, in_hbm = pl.BlockSpec(memory_space=pltpu.VMEM), pl.BlockSpec(memory_space=pl.ANY)
+    result = pl.pallas_call(
+        functools.partial(fused_kernel, ra_count, cb_count),
+        out_shape=jax.ShapeDtypeStruct((HALVES, rows, width), bf16),
+        in_specs=[in_vmem, in_vmem, in_hbm, in_hbm] + [in_vmem] * 4 + [in_hbm, in_vmem],
+        out_specs=in_vmem,
+        scratch_shapes=[
+            vmem((STAGED, width, CHUNK), f32),
+            vmem((STAGED, width, CHUNK), f32),
+            vmem((STAGED, CHUNK, width), f32),
+            vmem((chunks, width, 2 * CHUNK), bf16),
+            vmem((chunks, CHUNK, width), bf16),
+            vmem((layers + 1, HALVES, ra_count, z_block, width), bf16),
+            vmem((HALVES, rows, width), bf16),
+            vmem((HALVES, rows, LANES), f32),
+            vmem((rows + 8, 2 * CHUNK), f32),
+            vmem((chunks, 8, 2 * CHUNK), f32),
+            vmem((RING, x_count, block, 2 * CHUNK), bf16),
+            vmem((RING, x_count, block, 2 * CHUNK), bf16),
+            vmem((RING, x_count, block, 2 * CHUNK), f32),
+            vmem((RING, x_count, block, 2 * CHUNK), bf16),
+            vmem((RING, x_count, block, 2 * CHUNK), bf16),
+            vmem((RING, cb_count, block, CHUNK), bf16),
+            vmem((ra_count, z_block, width), f32),
+            vmem((parts, ra_count, z_block, width), bf16),
+            vmem((parts, ra_count, z_block, width), bf16),
+            vmem((parts, z_block, width), f32),
+            vmem((events, 8, rows), f32),
+            vmem((events, cb_count, 8, rows), f32),
+            dma((STAGED,)),
+            dma((STAGED,)),
+            dma((STAGED,)),
+            dma((RING,)),
+            dma((RING,)),
+            dma((RING, x_count)),
+            dma((RING, x_count)),
+            dma((RING, x_count)),
+            dma((RING, x_count)),
+            dma((RING,)),
+            dma((RING,)),
+            dma((parts, ra_count)),
+            dma((parts, ra_count)),
+            dma((parts, ra_count)),
+            dma((parts, ra_count)),
+            dma((events, cb_count)),
+            dma((events, cb_count)),
+        ],
+        compiler_params=pltpu.CompilerParams(
+            collective_id=0, has_side_effects=True, vmem_limit_bytes=62 * 1024 * 1024
+        ),
+        name="fused_sublayers",
+    )(
+        tokens.reshape(HALVES, rows, width),
+        norm_gains,
+        gate_weight,
+        value_weight,
+        gate_scale,
+        value_scale,
+        conv_gate,
+        conv_value,
+        down_weight,
+        down_scale,
+    )
+    return result.reshape(HALVES * rows, width)
+
+
 def solution(mesh):
     in_specs = (
         P("grp", "cb"),
@@ -91,5 +566,5 @@
     )
     out_specs = P("grp", "cb")
     return jax.shard_map(
-        on_device, mesh=mesh, in_specs=in_specs, out_specs=out_specs, check_vma=False
+        functools.partial(on_device_any, mesh.shape["ra"], mesh.shape["cb"]), mesh=mesh, in_specs=in_specs, out_specs=out_specs, check_vma=False
     )

time: 363 us -> 134 us (0.37)
  waiting for transfers between devices: 241 us -> 0 us
  Pallas kernels: 0 us -> 129 us
  other arithmetic: 41.6 us -> 0 us
  matrix products: 32.8 us -> 0 us
  blocking collectives: 22.7 us -> 0 us
  between operations: 13.7 us -> 0.01 us
  local copies, waits for them, and re-layouts: 10.5 us -> 4.95 us
    pallas_call x0 -> x1, Pallas kernels: none -> 129 us  [on_device_any(): pl.pallas_call(functools.partial(fused_kernel, ra_count, cb_count), out_s...]
    reduce_scatter x4 -> x0, waiting for transfers between devices: 111 us -> none  [the longest x2 77.4 us: on_device(): lax.psum_scatter(value_part, 'cb', scatter_dimension=1, tiled=True)]
    psum x2 -> x0, waiting for transfers between devices: 104 us -> none  [on_device(): down_total = lax.psum(partial_value, 'ra')]
    dot_general x6 -> x0, matrix products: 32.8 us -> none  [the longest x2 11.5 us: on_device(): jnp.dot(hidden, down_weight[layer_idx].astype(jnp.bfloat16), preferred_el...]
    another operation x3 -> x0, other arithmetic: 29.8 us -> none
    all_gather x2 -> x0, waiting for transfers between devices: 25.4 us -> none  [on_device(): hidden = lax.all_gather(hidden, 'cb', axis=1, tiled=True)]
    psum x3 -> x0, blocking collectives: 22.7 us -> none  [row_inverse(): lax.psum(jnp.sum(state_wide * state_wide, axis=1, keepdims=True), 'cb')]
    convert_element_type x3 -> x0, other arithmetic: 5.38 us -> none  [the longest x2 4.39 us: on_device(): hidden = (jax.nn.gelu(causal_taps(gate_pre, gate_taps), approximate=True)...]
  transfers between devices with their start and end apart: 8 -> 0, of which waited for: 8 -> 0; matrix products, arithmetic and copies ran while one was open for 9% -> 0% of each run, Pallas kernels for 0% -> 0%
where the time goes in v1:
time: 134 us
  Pallas kernels  129 us (96%)
  local copies, waits for them, and re-layouts  4.95 us (4%)
    pallas_call x1, Pallas kernels, on_device_any(): pl.pallas_call(functools.partial(fused_kernel, ra_count, cb_count), out_s...  129 us
    unnamed x3, local copies, waits for them, and re-layouts  4.95 us

profile of v1, /device:TPU:0, one launch (start us, length us, event | category | flops | bytes accessed | tf_op | source)
XLA Modules:
  0.0 133.9 jit_solution(17137138202579291333)
XLA Ops:
  0.0 1.5 %copy.11.conv_gate = f32[2,3,2816]{2,1,0:T(4,128)} copy(f32[2,3,2816]{2,0,1:T(2,128)} %param.16) | data formatting | bytes 135168 | tf_op args[6]
  1.5 1.5 %copy.12.conv_value = f32[2,3,2816]{2,1,0:T(4,128)} copy(f32[2,3,2816]{2,0,1:T(2,128)} %param.17) | data formatting | bytes 135168 | tf_op args[7]
  3.1 128.9 %fused_sublayers.1 = bf16[2,128,1024]{2,1,0:T(8,128)(2,1)} custom-call(bf16[2,128,1024]{2,1,0:T(8,128)(2,1)} %bitcast.3, f32[3,1024]{1,0:T(4,128)} %gains.1, f32[2,1024,2816]{2,1,0:T(8,128)} %gate_hbm.1, f32[2,1024,2816]{2,1,0:T(8,128)} %value_hbm.1, f32[2,2816]{1,0:T(2,128)} %gate_scale.1, f32[2,2816]{1,0:T(2,128)} %value_scale.1, ...), custom_call_target="tpu_custom_call" | custom-call | tf_op jit(solution)/shard_map/fused_sublayers/pallas_call | solution.py:489
  132.0 1.9 %copy.14 = bf16[256,1024]{1,0:T(8,128)(2,1)} copy(bf16[256,1024]{1,0:T(8,128)(2,1)} %bitcast.2) | data formatting | bytes 1048576

commit v2 on v1

--- a/solution.py
+++ b/solution.py
@@ -86,9 +86,9 @@
 CHUNK = 256
 RING = 12
 STAGED = 5
-BUBBLES = 4
-PAIR_SUM, GATED, PAIR_GATHER, DOWN = 1, 4, 7, 8
-Z_SUM, Z_GATHER, Z_SCALE = 4, 7, 8
+BUBBLES = 12
+PAIR_SUM, GATED, PAIR_GATHER, DOWN = 2, 5, 8, 10
+Z_SUM, Z_GATHER, Z_SCALE = 8, 13, 14
 
 
 def fused_kernel(

time: 134 us -> 113 us (0.84)
  Pallas kernels: 129 us -> 107 us
    pallas_call x1, Pallas kernels: 129 us -> 107 us  [on_device_any(): pl.pallas_call(functools.partial(fused_kernel, ra_count, cb_count), out_s...]
where the time goes in v2:
time: 113 us; the launch traced here: 112 us
  Pallas kernels  107 us (95%)
  local copies, waits for them, and re-layouts  4.95 us (4%)
    pallas_call x1, Pallas kernels, on_device_any(): pl.pallas_call(functools.partial(fused_kernel, ra_count, cb_count), out_s...  107 us
    unnamed x3, local copies, waits for them, and re-layouts  4.95 us

profile of v2, /device:TPU:0, one launch (start us, length us, event | category | flops | bytes accessed | tf_op | source)
XLA Modules:
  0.0 112.3 jit_solution(13095200637353050316)
XLA Ops:
  0.0 1.5 %copy.11.conv_gate = f32[2,3,2816]{2,1,0:T(4,128)} copy(f32[2,3,2816]{2,0,1:T(2,128)} %param.16) | data formatting | bytes 135168 | tf_op args[6]
  1.5 1.5 %copy.12.conv_value = f32[2,3,2816]{2,1,0:T(4,128)} copy(f32[2,3,2816]{2,0,1:T(2,128)} %param.17) | data formatting | bytes 135168 | tf_op args[7]
  3.1 107.3 %fused_sublayers.1 = bf16[2,128,1024]{2,1,0:T(8,128)(2,1)} custom-call(bf16[2,128,1024]{2,1,0:T(8,128)(2,1)} %bitcast.3, f32[3,1024]{1,0:T(4,128)} %gains.1, f32[2,1024,2816]{2,1,0:T(8,128)} %gate_hbm.1, f32[2,1024,2816]{2,1,0:T(8,128)} %value_hbm.1, f32[2,2816]{1,0:T(2,128)} %gate_scale.1, f32[2,2816]{1,0:T(2,128)} %value_scale.1, ...), custom_call_target="tpu_custom_call" | custom-call | tf_op jit(solution)/shard_map/fused_sublayers/pallas_call | solution.py:489
  110.4 1.9 %copy.14 = bf16[256,1024]{1,0:T(8,128)(2,1)} copy(bf16[256,1024]{1,0:T(8,128)(2,1)} %bitcast.2) | data formatting | bytes 1048576
